TPU v7x, 32 devices: a whole 2x2x4 slice. The times are simulated.
32 devices in a mesh: sp: 8 (over z, y), tp: 4 (over x, core).
Axes of the slice: x: 2, y: 2, z: 4, core: 2. Of those that a mesh axis runs over, the one named last changes fastest.
Arguments:
- hidden_in: bfloat16 [6144, 4096], P('sp', 'tp'), may hold values from -16 to 16
- norm_gain: bfloat16 [2, 4096], P(None, 'tp'), may hold values from 0.099609375 to 1.8984375
- value_proj: bfloat16 [2, 4096, 1024], P(None, 'tp', 'sp'), may hold values from -0.09375 to 0.09375
- gate_proj: bfloat16 [2, 4096, 1024], P(None, 'tp', 'sp'), may hold values from -0.09375 to 0.09375
- conv_taps: bfloat16 [2, 31, 1024], P(None, None, 'tp'), may hold values from -1 to 1
- conv_bias: bfloat16 [2, 1024], P(None, 'tp'), may hold values from -3 to 3
- group_gain: bfloat16 [2, 1024], P(None, 'tp'), may hold values from 0.099609375 to 1.8984375
- group_shift: bfloat16 [2, 1024], P(None, 'tp'), may hold values from -3 to 3
- out_proj: bfloat16 [2, 1024, 4096], P(None, 'sp', 'tp'), may hold values from -0.1875 to 0.1875
Outputs:
- hidden_out: bfloat16 [6144, 4096], P('sp', 'tp')
All inputs are finite; a program needn't handle non-finite values.
Results may differ from a plain program's by a relative error of at most 0.012.
Values may be sent and summed in bfloat16 or wider, within the bound.
A program may use at most 128 MiB of HBM per device.

v0:
```python
import jax
import jax.numpy as jnp
from jax import lax
from jax.sharding import PartitionSpec as P

D = 4096
C = 1024
GROUPS = 4
WIDTH = 31
row_floor = 1e-06
group_floor = 1e-05


def passed_along(value, axis, steps):
    count = lax.axis_size(axis)
    initial, last = (max(0, -steps), min(count, count - steps))
    return lax.ppermute(value, axis, [(source, source + steps) for source in range(initial, last)])


def rms_normed(residual_rows, gain_part):
    wide_rows = residual_rows.astype(jnp.float32)
    squares = lax.psum(jnp.sum(wide_rows * wide_rows, axis=1), "tp")
    scale_rows = lax.rsqrt(squares / D + row_floor)
    return (wide_rows * scale_rows[:, None] * gain_part.astype(jnp.float32)[None, :]).astype(
        jnp.bfloat16
    )


def gated_input(normed_rows, w_value, w_gate):
    numbers = (((0,), (1,)), ((), ()))
    value_part = lax.dot_general(w_value, normed_rows, numbers, preferred_element_type=jnp.float32)
    gate_part = lax.dot_general(w_gate, normed_rows, numbers, preferred_element_type=jnp.float32)
    summed = lax.psum_scatter(
        jnp.stack([value_part, gate_part], axis=1).astype(jnp.bfloat16),
        "tp",
        scatter_dimension=0,
        tiled=True,
    ).astype(jnp.float32)
    return (summed[:, 0] * jax.nn.sigmoid(summed[:, 1])).astype(jnp.bfloat16)


def depthwise(extended, taps_part, bias_part, out_len):
    widened = extended.astype(jnp.float32)
    taps = taps_part.astype(jnp.float32)
    filtered = (
        jnp.zeros((extended.shape[0], out_len), jnp.float32)
        + bias_part.astype(jnp.float32)[:, None]
    )
    for offset in range(WIDTH):
        filtered = filtered + taps[offset][:, None] * widened[:, offset : offset + out_len]
    return filtered


def group_normed(filtered, gain_part, shift_part, group_size):
    channels, out_len = filtered.shape
    grouped = filtered.reshape(channels // group_size, group_size, out_len)
    group_mean = jnp.mean(grouped, axis=1, keepdims=True)
    centered = grouped - group_mean
    group_var = jnp.mean(centered * centered, axis=1, keepdims=True)
    scaled = (centered * lax.rsqrt(group_var + group_floor)).reshape(channels, out_len)
    scaled = (
        scaled * gain_part.astype(jnp.float32)[:, None] + shift_part.astype(jnp.float32)[:, None]
    )
    return jax.nn.silu(scaled).astype(jnp.bfloat16)


def project_out(mixed, w_out):
    return lax.dot_general(
        lax.all_gather(mixed, "tp", axis=0, tiled=True),
        w_out,
        (((0,), (0,)), ((), ())),
        preferred_element_type=jnp.float32,
    )


def on_device(
    hidden_in,
    norm_gain,
    value_proj,
    gate_proj,
    conv_taps,
    conv_bias,
    group_gain,
    group_shift,
    out_proj,
):
    tok_rows = hidden_in.shape[0]
    layers = norm_gain.shape[0]
    reach_back = WIDTH - 1
    group_size = C // GROUPS
    all_value, all_gate, all_out = (
        lax.all_gather(value_proj, "sp", axis=2, tiled=True),
        lax.all_gather(gate_proj, "sp", axis=2, tiled=True),
        lax.all_gather(out_proj, "sp", axis=1, tiled=True),
    )
    residual_rows = hidden_in
    for level in range(layers):
        w_value, w_gate, w_out = (all_value[level], all_gate[level], all_out[level])
        normed_rows = rms_normed(residual_rows, norm_gain[level])
        gated = gated_input(normed_rows, w_value, w_gate)
        before = passed_along(gated[:, tok_rows - reach_back :], "sp", 1)
        extended = jnp.concatenate([before, gated], axis=1)
        out_len = extended.shape[1] - reach_back
        filtered = depthwise(extended, conv_taps[level], conv_bias[level], out_len)
        mixed = group_normed(filtered, group_gain[level], group_shift[level], group_size)
        update = project_out(mixed, w_out)
        kept_rows = residual_rows
        residual_rows = (kept_rows.astype(jnp.float32) + update).astype(jnp.bfloat16)
    return residual_rows


def solution(mesh):
    return jax.shard_map(
        on_device,
        mesh=mesh,
        in_specs=(
            P("sp", "tp"),
            P(None, "tp"),
            P(None, "tp", "sp"),
            P(None, "tp", "sp"),
            P(None, None, "tp"),
            P(None, "tp"),
            P(None, "tp"),
            P(None, "tp"),
            P(None, "sp", "tp"),
        ),
        out_specs=P("sp", "tp"),
        check_vma=False,
    )
```

profile of v0, /device:TPU:0, one launch (start us, length us, event | category | flops | bytes accessed | tf_op | source)
XLA Modules:
  0.0 397.9 jit_solution(1611705756857018403)
XLA Ops:
  8.1 1.8 fusion
  9.8 8.4 %psum.14 = f32[768]{0:T(1024)S(1)} all-reduce(f32[768]{0:T(1024)S(1)} %fusion), channel_id=1, replica_groups=mesh['sp'=8,'tp'=4] {'tp'}, use_global_device_ids=true, to_apply=%region_1.0 | all-reduce | flops 768 | bytes 6144 | tf_op jit(solution)/shard_map/psum | solution.py:22
  18.2 68.5 %all-gather.8.cloned.1.call-done = bf16[2,1024,1024]{2,1,0:T(8,128)(2,1)} async-done(((bf16[2,1024,128]{2,1,0:T(8,128)(2,1)}), bf16[2,1024,1024]{2,1,0:T(8,128)(2,1)}) %all-gather.8.cloned.1.call-update) | async-done | bytes 4194320 | tf_op jit(solution)/shard_map/all_gather | solution.py:93
  86.8 3.4 fusion.20
  90.2 71.4 %all-gather.6.cloned.1.call-done = bf16[2,1024,1024]{2,1,0:T(8,128)(2,1)} async-done(((bf16[2,1024,128]{2,1,0:T(8,128)(2,1)}), bf16[2,1024,1024]{2,1,0:T(8,128)(2,1)}) %all-gather.6.cloned.1.call-update) | async-done | bytes 4194320 | tf_op jit(solution)/shard_map/all_gather | solution.py:92
  161.7 3.4 fusion.21
  165.1 1.9 pad_maximum_fusion
  167.9 35.2 %reduce-scatter.3.cloned.1.call-done = bf16[256,2,768]{0,2,1:T(8,128)(2,1)} async-done(((bf16[1024,2,768]{0,2,1:T(8,128)(2,1)}), bf16[256,2,768]{0,2,1:T(8,128)(2,1)}) %reduce-scatter.3.cloned.1.call-update) | async-done | bytes 786448 | tf_op jit(solution)/shard_map/reduce_scatter | solution.py:33
  204.6 3.4 collective-permute-start
  208.0 1.4 collective-permute-done
  209.5 3.3 fusion.102
  214.3 63.7 %all-gather.12.cloned.1.call-done = bf16[2,1024,1024]{2,1,0:T(8,128)(2,1)} async-done(((bf16[2,128,1024]{2,1,0:T(8,128)(2,1)}), bf16[2,1024,1024]{2,1,0:T(8,128)(2,1)}) %all-gather.12.cloned.1.call-update) | async-done | bytes 4194320 | tf_op jit(solution)/shard_map/all_gather | solution.py:94
  278.0 19.8 %all-gather.10.cloned.1.call-done = bf16[1024,768]{0,1:T(8,128)(2,1)} async-done(((bf16[256,768]{0,1:T(8,128)(2,1)}), bf16[1024,768]{0,1:T(8,128)(2,1)}) %all-gather.10.cloned.1.call-update) | async-done | bytes 1572880 | tf_op jit(solution)/shard_map/all_gather | solution.py:69
  297.7 4.1 %fusion.4 = (f32[768]{0:T(1024)S(1)}, bf16[768,1024]{1,0:T(8,128)(2,1)S(1)}) fusion(bf16[1024,768]{0,1:T(8,128)(2,1)} %all-gather.10.cloned.1.call-done, bf16[2,1024,1024]{2,1,0:T(8,128)(2,1)} %all-gather.12.cloned.1.call-done, bf16[768,1024]{1,0:T(8,128)(2,1)S(1)} %copy-done), kind=kOutput, calls=%fused_computation.10 | convolution fusion | flops 1615330560 | bytes 6818816 | tf_op jit(solution)/shard_map/dot_general | solution.py:68
  301.8 5.9 %psum.15 = f32[768]{0:T(1024)S(1)} all-reduce(f32[768]{0:T(1024)S(1)} %get-tuple-element.81), channel_id=1, replica_groups=mesh['sp'=8,'tp'=4] {'tp'}, use_global_device_ids=true, to_apply=%region_6.7 | all-reduce | flops 768 | bytes 6144 | tf_op jit(solution)/shard_map/psum | solution.py:22
  307.7 3.6 fusion.19
  311.3 1.9 fusion.18
  313.2 2.0 pad_maximum_fusion.1
  315.2 38.9 %reduce-scatter.5.cloned.1.call-done = bf16[256,2,768]{0,2,1:T(8,128)(2,1)} async-done(((bf16[1024,2,768]{0,2,1:T(8,128)(2,1)}), bf16[256,2,768]{0,2,1:T(8,128)(2,1)}) %reduce-scatter.5.cloned.1.call-update) | async-done | bytes 786448 | tf_op jit(solution)/shard_map/reduce_scatter | solution.py:33
  355.6 3.4 collective-permute-start.1
  359.0 1.4 collective-permute-done.1
  360.5 3.3 fusion.100
  365.2 20.8 %all-gather.14.cloned.1.call-done = bf16[1024,768]{0,1:T(8,128)(2,1)} async-done(((bf16[256,768]{0,1:T(8,128)(2,1)}), bf16[1024,768]{0,1:T(8,128)(2,1)}) %all-gather.14.cloned.1.call-update) | async-done | bytes 1572880 | tf_op jit(solution)/shard_map/all_gather | solution.py:69
  386.0 5.0 %fusion.7 = bf16[768,1024]{1,0:T(8,128)(2,1)} fusion(bf16[768,1024]{1,0:T(8,128)(2,1)S(1)} %get-tuple-element.82, bf16[1024,768]{0,1:T(8,128)(2,1)} %all-gather.14.cloned.1.call-done, bf16[2,1024,1024]{2,1,0:T(8,128)(2,1)} %all-gather.12.cloned.1.call-done), kind=kOutput, calls=%fused_computation.13 | convolution fusion | flops 1612972032 | bytes 6815744 | tf_op jit(solution)/shard_map/dot_general | solution.py:68
  (55 shorter events, 8.4 us)
Async XLA Ops:
  6.5 80.2 %copy-start = (bf16[768,1024]{1,0:T(8,128)(2,1)S(1)}, bf16[768,1024]{1,0:T(8,128)(2,1)}, u32[]{:S(2)}) copy-start(bf16[768,1024]{1,0:T(8,128)(2,1)} %param.9) | copy-start | bytes 4718596
  6.5 11.7 %copy-start.2 = (bf16[2,1024]{1,0:T(2,128)(2,1)S(1)}, bf16[2,1024]{1,0:T(2,128)(2,1)}, u32[]{:S(2)}) copy-start(bf16[2,1024]{1,0:T(2,128)(2,1)} %param.10) | copy-start | bytes 12292
  6.5 80.2 %all-gather.8.cloned.1.call-start = ((), (), s32[]{:S(2)}) async-start(), calls=%async_computation.3 | async-start | bytes 4718592 | tf_op jit(solution)/shard_map/all_gather | solution.py:93
  7.3 154.4 %all-gather.6.cloned.1.call-start = ((), (), s32[]{:S(2)}) async-start(), calls=%async_computation.2 | async-start | bytes 4718592 | tf_op jit(solution)/shard_map/all_gather | solution.py:92
  8.0 195.1 %reduce-scatter.3.cloned.1.call-start = ((), (), s32[]{:S(2)}) async-start(), calls=%async_computation.4 | async-start | bytes 3932160 | tf_op jit(solution)/shard_map/reduce_scatter | solution.py:33
  167.0 0.7 copy-start.3
  167.0 0.7 copy-start.4
  167.0 0.8 copy-start.1
  167.1 110.9 %all-gather.12.cloned.1.call-start = ((), (), s32[]{:S(2)}) async-start(), calls=%async_computation.6 | async-start | bytes 4718592 | tf_op jit(solution)/shard_map/all_gather | solution.py:94
  167.6 130.1 %all-gather.10.cloned.1.call-start = ((), (), s32[]{:S(2)}) async-start(), calls=%async_computation.5 | async-start | bytes 1966080 | tf_op jit(solution)/shard_map/all_gather | solution.py:69
  167.9 40.1 %copy-start.5 = (bf16[2,256]{1,0:T(2,128)(2,1)S(1)}, bf16[2,256]{1,0:T(2,128)(2,1)}, u32[]{:S(2)}) copy-start(bf16[2,256]{1,0:T(2,128)(2,1)} %param.16) | copy-start | bytes 3076
  204.6 4.8 %collective-permute-start = (bf16[256,30]{0,1:T(8,128)(2,1)S(1)}, bf16[256,30]{0,1:T(8,128)(2,1)S(1)}, u32[]{:S(2)}, u32[]{:S(2)}) collective-permute-start(bf16[256,30]{0,1:T(8,128)(2,1)S(1)} %slice.651), channel_id=1, source_target_pairs={{0,4},{4,8},{8,12},{12,16},{16,20},{20,24},{24,28},{1,5},{5,9},{9,... | collective-permute-start | bytes 46088 | tf_op jit(solution)/shard_map/ppermute | solution.py:17
  214.2 139.9 %reduce-scatter.5.cloned.1.call-start = ((), (), s32[]{:S(2)}) async-start(), calls=%async_computation.7 | async-start | bytes 3932160 | tf_op jit(solution)/shard_map/reduce_scatter | solution.py:33
  307.7 3.6 copy-start.6
  315.2 70.9 %all-gather.14.cloned.1.call-start = ((), (), s32[]{:S(2)}) async-start(), calls=%async_computation.8 | async-start | bytes 1966080 | tf_op jit(solution)/shard_map/all_gather | solution.py:69
  355.6 4.8 %collective-permute-start.1 = (bf16[256,30]{0,1:T(8,128)(2,1)S(1)}, bf16[256,30]{0,1:T(8,128)(2,1)S(1)}, u32[]{:S(2)}, u32[]{:S(2)}) collective-permute-start(bf16[256,30]{0,1:T(8,128)(2,1)S(1)} %slice.719), channel_id=1, source_target_pairs={{0,4},{4,8},{8,12},{12,16},{16,20},{20,24},{24,28},{1,5},{5,9},{9,... | collective-permute-start | bytes 46088 | tf_op jit(solution)/shard_map/ppermute | solution.py:17
Sparse Core Ops, SparseCore 0:
  9.4 77.3 all-gather.7
  88.8 72.8 all-gather.5
  167.2 35.8 reduce-scatter.2
  205.1 72.7 all-gather.11
  279.4 18.3 all-gather.9
  315.3 38.7 reduce-scatter.4
  365.3 20.6 all-gather.13
where the time goes:
time: 398 us
  waiting for transfers between devices  323 us (81%)
  matrix products  21.4 us (5%)
  other arithmetic  18.2 us (5%)
  blocking collectives  14.3 us (4%)
  between operations  13.7 us (3%)
  starting transfers between devices  7.01 us (2%)
    reduce_scatter x2, waiting for transfers between devices, gated_input(): lax.psum_scatter(jnp.stack([value_part, gate_part], axis=1).astype(jnp.bf...  74.1 us
    all_gather x1, waiting for transfers between devices, on_device(): lax.all_gather(value_proj, 'sp', axis=2, tiled=True)  71.4 us
    all_gather x1, waiting for transfers between devices, on_device(): lax.all_gather(gate_proj, 'sp', axis=2, tiled=True)  68.5 us
    all_gather x1, waiting for transfers between devices, on_device(): lax.all_gather(out_proj, 'sp', axis=1, tiled=True)  63.7 us
    all_gather x2, waiting for transfers between devices, project_out(): lax.all_gather(mixed, 'tp', axis=0, tiled=True)  40.6 us
    psum x2, blocking collectives, rms_normed(): squares = lax.psum(jnp.sum(wide_rows * wide_rows, axis=1), 'tp')  14.3 us
    dot_general x2, matrix products, project_out(): lax.dot_general(lax.all_gather(mixed, 'tp', axis=0, tiled=True), w_out, (...  9.1 us
  transfers between devices with their start and end apart: 9, of which 9 were waited for; matrix products, arithmetic and copies ran while one was open for 3% of the time, Pallas kernels for 0%

commit v1 on v0

--- a/solution.py
+++ b/solution.py
@@ -88,9 +88,10 @@
     layers = norm_gain.shape[0]
     reach_back = WIDTH - 1
     group_size = C // GROUPS
+    face_launch = lambda sheet: jnp.concatenate(lax.all_gather(sheet, "sp"), axis=2)
     all_value, all_gate, all_out = (
         lax.all_gather(value_proj, "sp", axis=2, tiled=True),
-        lax.all_gather(gate_proj, "sp", axis=2, tiled=True),
+        face_launch(gate_proj),
         lax.all_gather(out_proj, "sp", axis=1, tiled=True),
     )
     residual_rows = hidden_in

time: 398 us -> 399 us (level)
  waiting for transfers between devices: 323 us -> 309 us
  local copies, waits for them, and re-layouts: 0.2 us -> 10.8 us
    slice x0 -> x3, local copies, waits for them, and re-layouts: none -> 10.6 us  [on_device(): w_value, w_gate, w_out = (all_value[level], all_gate[level], all_out[level])]
    all_gather x1, waiting for transfers between devices: 71.4 us -> 62.1 us  [on_device(): lax.all_gather(value_proj, 'sp', axis=2, tiled=True)]
  transfers between devices with their start and end apart: 9 -> 9, of which waited for: 9 -> 9; matrix products, arithmetic and copies ran while one was open for 3% -> 6% of each run, Pallas kernels for 0% -> 0%
where the time goes in v1:
time: 399 us; the launch traced here: 398 us
  waiting for transfers between devices  309 us (77%)
  matrix products  25 us (6%)
  other arithmetic  18.2 us (5%)
  blocking collectives  14.2 us (4%)
  between operations  13.8 us (3%)
  local copies, waits for them, and re-layouts  10.8 us (3%)
  starting transfers between devices  7.03 us (2%)
    reduce_scatter x2, waiting for transfers between devices, gated_input(): lax.psum_scatter(jnp.stack([value_part, gate_part], axis=1).astype(jnp.bf...  74.1 us
    all_gather x1, waiting for transfers between devices, on_device(): lax.all_gather(sheet, 'sp')  66.8 us
    all_gather x1, waiting for transfers between devices, on_device(): lax.all_gather(value_proj, 'sp', axis=2, tiled=True)  62.1 us
    all_gather x1, waiting for transfers between devices, on_device(): lax.all_gather(out_proj, 'sp', axis=1, tiled=True)  61 us
    all_gather x2, waiting for transfers between devices, project_out(): lax.all_gather(mixed, 'tp', axis=0, tiled=True)  40.6 us
    psum x2, blocking collectives, rms_normed(): squares = lax.psum(jnp.sum(wide_rows * wide_rows, axis=1), 'tp')  14.2 us
    slice x3, local copies, waits for them, and re-layouts, on_device(): w_value, w_gate, w_out = (all_value[level], all_gate[level], all_out[level])  10.6 us
    dot_general x2, matrix products, project_out(): lax.dot_general(lax.all_gather(mixed, 'tp', axis=0, tiled=True), w_out, (...  10.5 us
  transfers between devices with their start and end apart: 9, of which 9 were waited for; matrix products, arithmetic and copies ran while one was open for 6% of the time, Pallas kernels for 0%

profile of v1, /device:TPU:0, one launch (start us, length us, event | category | flops | bytes accessed | tf_op | source)
XLA Modules:
  0.0 398.4 jit_solution(14979419980086740624)
XLA Ops:
  9.8 8.4 %psum.14 = f32[768]{0:T(1024)S(1)} all-reduce(f32[768]{0:T(1024)S(1)} %fusion), channel_id=1, replica_groups=mesh['sp'=8,'tp'=4] {'tp'}, use_global_device_ids=true, to_apply=%region_1.0 | all-reduce | flops 768 | bytes 6144 | tf_op jit(solution)/shard_map/psum | solution.py:22
  18.2 66.8 %all-gather.15.cloned.1.call-done = bf16[16,1024,128]{2,1,0:T(8,128)(2,1)} async-done(((bf16[2,1024,128]{2,1,0:T(8,128)(2,1)}), bf16[16,1024,128]{2,1,0:T(8,128)(2,1)}) %all-gather.15.cloned.1.call-update) | async-done | bytes 4194320 | tf_op jit(solution)/shard_map/all_gather | solution.py:91
  85.0 3.9 fusion.100
  89.0 3.9 copy.12
  92.9 5.2 %fusion.14 = bf16[1024,1,768]{0,2,1:T(8,128)(2,1)} fusion(bf16[1024,1024]{0,1:T(8,128)(2,1)} %bitcast.127, bf16[768,1024]{1,0:T(8,128)(2,1)} %param.9, f32[1024]{0:T(1024)S(1)} %bitcast.134, f32[768]{0:T(1024)S(1)} %add_rsqrt_fusion.3), kind=kOutput, calls=%fused_computation.28 | convolution fusion | flops 1614544896 | bytes 5250048 | tf_op jit(solution)/shard_map/dot_general | solution.py:32
  98.1 62.1 %all-gather.7.cloned.1.call-done = bf16[2,1024,1024]{2,1,0:T(8,128)(2,1)} async-done(((bf16[2,1024,128]{2,1,0:T(8,128)(2,1)}), bf16[2,1024,1024]{2,1,0:T(8,128)(2,1)}) %all-gather.7.cloned.1.call-update) | async-done | bytes 4194320 | tf_op jit(solution)/shard_map/all_gather | solution.py:93
  160.3 4.0 %fusion.17 = bf16[1024,1,768]{0,2,1:T(8,128)(2,1)S(1)} fusion(bf16[2,1024,1024]{2,1,0:T(8,128)(2,1)} %all-gather.7.cloned.1.call-done, bf16[768,1024]{1,0:T(8,128)(2,1)} %param.9, f32[1024]{0:T(1024)S(1)} %bitcast.135, f32[768]{0:T(1024)S(1)} %add_rsqrt_fusion.3), kind=kOutput, calls=%fused_computation.31 | convolution fusion | flops 1614544896 | bytes 5250048 | tf_op jit(solution)/shard_map/dot_general | solution.py:31
  164.3 2.0 pad_maximum_fusion
  167.2 35.2 %reduce-scatter.3.cloned.1.call-done = bf16[256,2,768]{0,2,1:T(8,128)(2,1)} async-done(((bf16[1024,2,768]{0,2,1:T(8,128)(2,1)}), bf16[256,2,768]{0,2,1:T(8,128)(2,1)}) %reduce-scatter.3.cloned.1.call-update) | async-done | bytes 786448 | tf_op jit(solution)/shard_map/reduce_scatter | solution.py:33
  203.9 3.4 collective-permute-start
  208.8 3.3 fusion.98
  213.5 2.7 copy.13
  216.3 61.0 %all-gather.11.cloned.1.call-done = bf16[2,1024,1024]{2,1,0:T(8,128)(2,1)} async-done(((bf16[2,128,1024]{2,1,0:T(8,128)(2,1)}), bf16[2,1024,1024]{2,1,0:T(8,128)(2,1)}) %all-gather.11.cloned.1.call-update) | async-done | bytes 4194320 | tf_op jit(solution)/shard_map/all_gather | solution.py:95
  277.2 19.8 %all-gather.9.cloned.1.call-done = bf16[1024,768]{0,1:T(8,128)(2,1)} async-done(((bf16[256,768]{0,1:T(8,128)(2,1)}), bf16[1024,768]{0,1:T(8,128)(2,1)}) %all-gather.9.cloned.1.call-update) | async-done | bytes 1572880 | tf_op jit(solution)/shard_map/all_gather | solution.py:69
  297.0 5.5 %fusion.4 = (f32[768]{0:T(1024)S(1)}, bf16[768,1024]{1,0:T(8,128)(2,1)}) fusion(bf16[1024,768]{0,1:T(8,128)(2,1)} %all-gather.9.cloned.1.call-done, bf16[2,1024,1024]{2,1,0:T(8,128)(2,1)} %all-gather.11.cloned.1.call-done, bf16[768,1024]{1,0:T(8,128)(2,1)} %param.9), kind=kOutput, calls=%fused_computation.10 | convolution fusion | flops 1615330560 | bytes 6818816 | tf_op jit(solution)/shard_map/dot_general | solution.py:68
  302.5 5.9 %psum.15 = f32[768]{0:T(1024)S(1)} all-reduce(f32[768]{0:T(1024)S(1)} %get-tuple-element.83), channel_id=1, replica_groups=mesh['sp'=8,'tp'=4] {'tp'}, use_global_device_ids=true, to_apply=%region_6.7 | all-reduce | flops 768 | bytes 6144 | tf_op jit(solution)/shard_map/psum | solution.py:22
  308.4 3.4 fusion.15
  311.9 1.8 fusion.16
  313.7 1.9 pad_maximum_fusion.1
  315.7 38.9 %reduce-scatter.5.cloned.1.call-done = bf16[256,2,768]{0,2,1:T(8,128)(2,1)} async-done(((bf16[1024,2,768]{0,2,1:T(8,128)(2,1)}), bf16[256,2,768]{0,2,1:T(8,128)(2,1)}) %reduce-scatter.5.cloned.1.call-update) | async-done | bytes 786448 | tf_op jit(solution)/shard_map/reduce_scatter | solution.py:33
  356.1 3.4 collective-permute-start.1
  361.0 3.3 fusion.96
  365.7 20.8 %all-gather.13.cloned.1.call-done = bf16[1024,768]{0,1:T(8,128)(2,1)} async-done(((bf16[256,768]{0,1:T(8,128)(2,1)}), bf16[1024,768]{0,1:T(8,128)(2,1)}) %all-gather.13.cloned.1.call-update) | async-done | bytes 1572880 | tf_op jit(solution)/shard_map/all_gather | solution.py:69
  386.5 5.0 %fusion.7 = bf16[768,1024]{1,0:T(8,128)(2,1)} fusion(bf16[768,1024]{1,0:T(8,128)(2,1)S(1)} %copy-done.9, bf16[1024,768]{0,1:T(8,128)(2,1)} %all-gather.13.cloned.1.call-done, bf16[2,1024,1024]{2,1,0:T(8,128)(2,1)} %all-gather.11.cloned.1.call-done), kind=kOutput, calls=%fused_computation.13 | convolution fusion | flops 1612972032 | bytes 6815744 | tf_op jit(solution)/shard_map/dot_general | solution.py:68
  (64 shorter events, 13.0 us)
Async XLA Ops:
  6.5 11.7 %copy-start.3 = (bf16[2,1024]{1,0:T(2,128)(2,1)S(1)}, bf16[2,1024]{1,0:T(2,128)(2,1)}, u32[]{:S(2)}) copy-start(bf16[2,1024]{1,0:T(2,128)(2,1)} %param.10) | copy-start | bytes 12292
  6.5 78.5 %all-gather.15.cloned.1.call-start = ((), (), s32[]{:S(2)}) async-start(), calls=%async_computation.8 | async-start | bytes 4718592 | tf_op jit(solution)/shard_map/all_gather | solution.py:91
  7.3 153.0 %all-gather.7.cloned.1.call-start = ((), (), s32[]{:S(2)}) async-start(), calls=%async_computation.2 | async-start | bytes 4718592 | tf_op jit(solution)/shard_map/all_gather | solution.py:93
  8.0 194.4 %reduce-scatter.3.cloned.1.call-start = ((), (), s32[]{:S(2)}) async-start(), calls=%async_computation.3 | async-start | bytes 3932160 | tf_op jit(solution)/shard_map/reduce_scatter | solution.py:33
  160.3 4.0 %copy-start.1 = (bf16[1024,1,768]{0,2,1:T(8,128)(2,1)S(1)}, bf16[1024,1,768]{0,2,1:T(8,128)(2,1)}, u32[]{:S(2)}) copy-start(bf16[1024,1,768]{0,2,1:T(8,128)(2,1)} %fusion.14) | copy-start | bytes 4718596
  166.3 0.7 copy-start.4
  166.3 0.7 copy-start.5
  166.3 0.8 copy-start.2
  166.3 110.9 %all-gather.11.cloned.1.call-start = ((), (), s32[]{:S(2)}) async-start(), calls=%async_computation.5 | async-start | bytes 4718592 | tf_op jit(solution)/shard_map/all_gather | solution.py:95
  166.9 130.1 %all-gather.9.cloned.1.call-start = ((), (), s32[]{:S(2)}) async-start(), calls=%async_computation.4 | async-start | bytes 1966080 | tf_op jit(solution)/shard_map/all_gather | solution.py:69
  167.2 40.1 %copy-start.6 = (bf16[2,256]{1,0:T(2,128)(2,1)S(1)}, bf16[2,256]{1,0:T(2,128)(2,1)}, u32[]{:S(2)}) copy-start(bf16[2,256]{1,0:T(2,128)(2,1)} %param.16) | copy-start | bytes 3076
  203.9 4.8 %collective-permute-start = (bf16[256,30]{0,1:T(8,128)(2,1)S(1)}, bf16[256,30]{0,1:T(8,128)(2,1)S(1)}, u32[]{:S(2)}, u32[]{:S(2)}) collective-permute-start(bf16[256,30]{0,1:T(8,128)(2,1)S(1)} %slice.653), channel_id=1, source_target_pairs={{0,4},{4,8},{8,12},{12,16},{16,20},{20,24},{24,28},{1,5},{5,9},{9,... | collective-permute-start | bytes 46088 | tf_op jit(solution)/shard_map/ppermute | solution.py:17
  213.5 141.1 %reduce-scatter.5.cloned.1.call-start = ((), (), s32[]{:S(2)}) async-start(), calls=%async_computation.6 | async-start | bytes 3932160 | tf_op jit(solution)/shard_map/reduce_scatter | solution.py:33
  216.3 92.2 %copy-start = (bf16[1,1024,8,128]{1,3,2,0:T(8,128)(2,1)S(1)}, bf16[1,1024,8,128]{1,3,2,0:T(8,128)(2,1)}, u32[]{:S(2)}) copy-start(bf16[1,1024,8,128]{1,3,2,0:T(8,128)(2,1)} %copy.13) | copy-start | bytes 6291460
  308.4 3.4 copy-start.7
  308.4 3.4 copy-start.8
  315.7 70.9 %all-gather.13.cloned.1.call-start = ((), (), s32[]{:S(2)}) async-start(), calls=%async_computation.7 | async-start | bytes 1966080 | tf_op jit(solution)/shard_map/all_gather | solution.py:69
  356.1 4.8 %collective-permute-start.1 = (bf16[256,30]{0,1:T(8,128)(2,1)S(1)}, bf16[256,30]{0,1:T(8,128)(2,1)S(1)}, u32[]{:S(2)}, u32[]{:S(2)}) collective-permute-start(bf16[256,30]{0,1:T(8,128)(2,1)S(1)} %slice.721), channel_id=1, source_target_pairs={{0,4},{4,8},{8,12},{12,16},{16,20},{20,24},{24,28},{1,5},{5,9},{9,... | collective-permute-start | bytes 46088 | tf_op jit(solution)/shard_map/ppermute | solution.py:17
  364.3 22.2 %copy-start.9 = (bf16[768,1024]{1,0:T(8,128)(2,1)S(1)}, bf16[768,1024]{1,0:T(8,128)(2,1)}, u32[]{:S(2)}) copy-start(bf16[768,1024]{1,0:T(8,128)(2,1)} %get-tuple-element.84) | copy-start | bytes 4718596
Sparse Core Ops, SparseCore 0:
  9.5 75.5 all-gather.14
  87.0 73.1 all-gather.6
  166.4 35.8 reduce-scatter.2
  204.4 72.7 all-gather.10
  278.6 18.3 all-gather.8
  315.8 38.7 reduce-scatter.4
  365.9 20.6 all-gather.12
